TPU v7x, 32 devices: a whole 2x2x4 slice. The times are simulated.
32 devices in a mesh: kv: 4 (over y, x), tp: 8 (over z, core).
Axes of the slice: x: 2, y: 2, z: 4, core: 2. Of those that a mesh axis runs over, the one named last changes fastest.
Arguments:
- tokens: bfloat16 [384, 4096], P('kv', 'tp'), may hold values from -20 to 20
- state: float32 [384, 32, 4096], P('kv', 'tp'), may hold values from -4 to 4
- w_query: bfloat16 [4096, 2048], P(None, 'tp'), may hold values from -0.09375 to 0.09375
- w_key: bfloat16 [4096, 2048], P(None, 'tp'), may hold values from -0.09375 to 0.09375
- w_value: bfloat16 [4096, 2048], P(None, 'tp'), may hold values from -0.09375 to 0.09375
- w_gate: bfloat16 [4096, 2048], P(None, 'tp'), may hold values from -0.09375 to 0.09375
- w_decay: bfloat16 [4096, 32], replicated, may hold values from -0.09375 to 0.09375
- w_beta: bfloat16 [4096, 32], replicated, may hold values from -0.09375 to 0.09375
- decay_rate: float32 [32], P('tp'), may hold values from 0.03 to 3
- decay_bias: float32 [32], P('tp'), may hold values from -1 to 1
- mix_gain: float32 [4096], replicated, may hold values from 0.1 to 1.9
- out_gain: float32 [64], replicated, may hold values from 0.1 to 1.9
- w_out: bfloat16 [2048, 4096], P('tp'), may hold values from -0.125 to 0.125
- ffn_gain: float32 [4096], replicated, may hold values from 0.1 to 1.9
- w_up: bfloat16 [4096, 16384], P('tp', 'kv'), may hold values from -0.09375 to 0.09375
- w_down: bfloat16 [16384, 4096], P('kv', 'tp'), may hold values from -0.046875 to 0.046875
Outputs:
- mixed: bfloat16 [384, 4096], P('kv', 'tp')
- new_state: float32 [384, 32, 4096], P('kv', 'tp')
All inputs are finite; a program needn't handle non-finite values.
Results may differ from a plain program's by a relative error of at most 0.024.
Values may be sent and summed in bfloat16 or wider, within the bound.
A program may use at most 128 MiB of HBM per device.

v0:
```python
import jax
import jax.numpy as jnp
from jax import lax
from jax.sharding import PartitionSpec as P

D = 4096
HEAD_DIM = 64


EPS = 1e-06


def unit_norm(vector):
    return vector * lax.rsqrt(jnp.sum(vector * vector, axis=-1, keepdims=True) + EPS)


def local(
    tokens,
    state,
    w_query,
    w_key,
    w_value,
    w_gate,
    w_decay,
    w_beta,
    decay_rate,
    decay_bias,
    mix_gain,
    out_gain,
    w_out,
    ffn_gain,
    w_up,
    w_down,
):
    rows = tokens.shape[0]
    width_share = tokens.shape[1]
    head_count = w_query.shape[1] // HEAD_DIM
    full_rows = lax.all_gather(tokens, "tp", axis=1, tiled=True)
    full_f = full_rows.astype(jnp.float32)
    normed = (
        full_f * lax.rsqrt(jnp.mean(full_f * full_f, axis=-1, keepdims=True) + EPS) * mix_gain
    ).astype(jnp.bfloat16)
    query = jnp.dot(normed, w_query, preferred_element_type=jnp.float32).reshape(
        rows, head_count, HEAD_DIM
    )
    key_proj = jnp.dot(normed, w_key, preferred_element_type=jnp.float32).reshape(
        rows, head_count, HEAD_DIM
    )
    value = jnp.dot(normed, w_value, preferred_element_type=jnp.float32).reshape(
        rows, head_count, HEAD_DIM
    )
    gate = jnp.dot(normed, w_gate, preferred_element_type=jnp.float32).reshape(
        rows, head_count, HEAD_DIM
    )
    query = unit_norm(query) * HEAD_DIM ** (-0.5)
    key_proj = unit_norm(key_proj)
    head_start = lax.axis_index("tp") * head_count
    decay_cols = lax.dynamic_slice_in_dim(w_decay, head_start, head_count, 1)
    beta_cols = lax.dynamic_slice_in_dim(w_beta, head_start, head_count, 1)
    pre_decay = jnp.dot(normed, decay_cols, preferred_element_type=jnp.float32)
    decay = jnp.exp(-decay_rate * jax.nn.softplus(pre_decay + decay_bias))
    strength = jax.nn.sigmoid(jnp.dot(normed, beta_cols, preferred_element_type=jnp.float32))
    matrix = state.reshape(rows, head_count, HEAD_DIM, HEAD_DIM) * decay[:, :, None, None]
    recalled = jnp.einsum("bhk,bhkv->bhv", key_proj, matrix, precision=lax.Precision.HIGHEST)
    delta = (value - recalled) * strength[:, :, None]
    matrix = matrix + key_proj[:, :, :, None] * delta[:, :, None, :]
    head_out = jnp.einsum("bhk,bhkv->bhv", query, matrix, precision=lax.Precision.HIGHEST)
    head_out = (
        head_out
        * lax.rsqrt(jnp.mean(head_out * head_out, axis=-1, keepdims=True) + EPS)
        * out_gain
        * jax.nn.silu(gate)
    )
    head_out = head_out.reshape(rows, head_count * HEAD_DIM).astype(jnp.bfloat16)
    partial_value = jnp.dot(head_out, w_out, preferred_element_type=jnp.float32)
    feature_start = lax.axis_index("tp") * width_share
    gain_share = lax.dynamic_slice_in_dim(ffn_gain, feature_start, width_share, 0)
    resid = tokens.astype(jnp.float32) + lax.psum_scatter(
        partial_value.astype(jnp.bfloat16), "tp", scatter_dimension=1, tiled=True
    ).astype(jnp.float32)
    squares = lax.psum(jnp.sum(resid * resid, axis=-1), "tp")
    scale = lax.rsqrt(squares[:, None] / D + EPS)
    ffn_in = (resid * scale * gain_share).astype(jnp.bfloat16)
    up_part = jnp.dot(
        lax.all_gather(ffn_in, "kv", axis=0, tiled=True), w_up, preferred_element_type=jnp.float32
    )
    up_full = lax.psum(up_part.astype(jnp.bfloat16), "tp").astype(jnp.float32)
    hidden = jnp.square(jax.nn.relu(up_full)).astype(jnp.bfloat16)
    down = lax.psum_scatter(
        jnp.dot(hidden, w_down, preferred_element_type=jnp.float32).astype(jnp.bfloat16),
        "kv",
        scatter_dimension=0,
        tiled=True,
    ).astype(jnp.float32)
    mixed = (resid + down).astype(jnp.bfloat16)
    return (mixed, matrix.reshape(rows, head_count, HEAD_DIM * HEAD_DIM))


def solution(mesh):
    in_specs = (
        P("kv", "tp"),
        P("kv", "tp", None),
        P(None, "tp"),
        P(None, "tp"),
        P(None, "tp"),
        P(None, "tp"),
        P(),
        P(),
        P("tp"),
        P("tp"),
        P(),
        P(),
        P("tp", None),
        P(),
        P("tp", "kv"),
        P("kv", "tp"),
    )
    out_specs = (P("kv", "tp"), P("kv", "tp", None))
    return jax.shard_map(local, mesh=mesh, in_specs=in_specs, out_specs=out_specs, check_vma=False)
```

profile of v0, /device:TPU:24, one launch (start us, length us, event | category | flops | bytes accessed | tf_op | source)
XLA Modules:
  0.0 232.1 jit_solution(16335360079471447695)
XLA Ops:
  7.2 0.0 copy-start
  7.2 0.0 reduce-scatter.3.cloned.1.call-start
  7.2 0.8 neg.14
  8.0 15.9 %all_gather.6 = bf16[96,4096]{1,0:T(8,128)(2,1)S(1)} all-gather(bf16[96,512]{1,0:T(8,128)(2,1)} %param.16), channel_id=1, replica_groups=mesh['kv'=4,'tp'=8] {'tp'}, dimensions={1}, use_global_device_ids=true | all-gather | bytes 884736 | tf_op jit(solution)/shard_map/all_gather | solution.py:38
  23.9 0.0 copy-start.6
  23.9 0.0 copy-start.9
  23.9 0.3 fusion.2
  24.2 2.7 %fusion.21 = f32[96,256]{0,1:T(8,128)S(1)} fusion(bf16[4096,256]{1,0:T(8,128)(2,1)} %param.20, bf16[96,4096]{1,0:T(8,128)(2,1)S(1)} %all_gather.6, f32[4096]{0:T(1024)} %param.26, f32[96]{0:T(128)S(1)} %add_rsqrt_fusion.4), kind=kOutput, calls=%fused_computation.45 | convolution fusion | flops 202899456 | bytes 2998656 | tf_op jit(solution)/shard_map/dot_general | solution.py:49
  26.9 0.0 copy-done.6
  26.9 0.0 copy-done.9
  26.9 0.0 copy-start.7
  26.9 1.0 fusion.18
  27.9 0.6 copy-done.7
  28.5 0.0 copy-start.8
  28.5 1.0 multiply_reduce_fusion.4
  29.5 0.6 copy-done.8
  30.1 1.0 multiply_reduce_fusion.5
  31.1 0.0 copy-start.10
  31.1 9.2 %copy.22 = f32[96,4,4096]{0,2,1:T(8,128)} copy(f32[96,4,4096]{2,1,0:T(4,128)} %param.17) | data formatting | bytes 12582912 | tf_op args[1]
  40.3 1.2 fusion.8
  41.6 0.0 copy-done.10
  41.6 1.2 fusion.12
  42.8 0.0 copy-start.2
  42.8 5.0 %multiply_reduce_fusion.1 = f32[96,4,64]{0,2,1:T(8,128)S(1)} fusion(f32[96,4,64,64]{0,3,2,1:T(8,128)} %bitcast.21, f32[96,4,64]{0,2,1:T(8,128)S(1)} %broadcast_multiply_fusion.1, f32[96,4]{0,1:T(4,128)S(1)} %fusion.12), kind=kLoop, calls=%fused_computation.2 | loop fusion | flops 4694016 | bytes 6489600 | tf_op jit(solution)/shard_map/bhk,bhkv->bhv/dot_general | solution.py:64
  47.9 0.7 copy-done.2
  48.6 0.0 copy-start.5
  48.6 4.2 %broadcast_multiply_fusion = (f32[96,4,64,64]{0,3,2,1:T(8,128)}, f32[96,4,64]{0,2,1:T(8,128)S(1)}) fusion(f32[96,4,64]{0,2,1:T(8,128)S(1)} %get-tuple-element.10, f32[96,4,64]{0,2,1:T(8,128)S(1)} %broadcast_multiply_fusion.1, f32[96,4,64,64]{0,3,2,1:T(8,128)S(1)} %bitcast.22, f32[96,4]{0,1:T(4,128)S(1)} %fusion.12, f32[96,4,64]{0,2,1:T(8,128)S(1)} %get-tuple-element.11), kind=kLoop, calls=%fused_computation.6 | loop fusion | flops 7839744 | bytes 12977664 | tf_op jit(solution)/shard_map/mul | solution.py:66
  52.8 0.0 copy-start.3
  52.8 0.0 copy-done.5
  52.9 0.1 multiply_convert_fusion.5
  52.9 0.0 copy-done
  53.0 1.4 convolution_convert_fusion.1
  54.3 0.0 reduce-scatter.3.cloned.1.call-update
  54.4 0.0 all-reduce.2.cloned.1.call-start
  54.4 0.8 dynamic_slice.11
  55.2 28.6 %reduce-scatter.3.cloned.1.call-done = bf16[96,512]{1,0:T(8,128)(2,1)} async-done(((bf16[96,4096]{1,0:T(8,128)(2,1)}), bf16[96,512]{1,0:T(8,128)(2,1)}) %reduce-scatter.3.cloned.1.call-update) | async-done | bytes 98320 | tf_op jit(solution)/shard_map/reduce_scatter | solution.py:78
  83.8 0.0 copy-done.3
  83.8 1.0 multiply_reduce_fusion.2
  84.8 13.2 %psum.14 = f32[96]{0:T(128)S(1)} all-reduce(f32[96]{0:T(128)S(1)} %multiply_reduce_fusion.2), channel_id=1, replica_groups=mesh['kv'=4,'tp'=8] {'tp'}, use_global_device_ids=true, to_apply=%region_6.7 | all-reduce | flops 96 | bytes 768 | tf_op jit(solution)/shard_map/psum | solution.py:81
  98.0 1.0 multiply_convert_fusion.4
  99.0 10.4 %all_gather.7 = bf16[384,512]{1,0:T(8,128)(2,1)S(1)} all-gather(bf16[96,512]{1,0:T(8,128)(2,1)S(1)} %multiply_convert_fusion.4), channel_id=1, replica_groups=mesh['kv'=4,'tp'=8] {'kv'}, dimensions={0}, use_global_device_ids=true | all-gather | bytes 491520 | tf_op jit(solution)/shard_map/all_gather | solution.py:85
  109.4 5.7 %convolution_convert_fusion = bf16[384,4096]{1,0:T(8,128)(2,1)} fusion(bf16[384,512]{1,0:T(8,128)(2,1)S(1)} %all_gather.7, bf16[512,4096]{1,0:T(8,128)(2,1)} %param.30), kind=kOutput, calls=%fused_computation.4 | convolution fusion | flops 1612185600 | bytes 7733248 | tf_op jit(solution)/shard_map/dot_general | solution.py:84
  115.0 0.0 all-reduce.2.cloned.1.call-update
  115.1 0.2 reduce-scatter.5.cloned.1.call-start
  115.3 77.2 %all-reduce.2.cloned.1.call-done = bf16[384,4096]{1,0:T(8,128)(2,1)} async-done(((bf16[384,4096]{1,0:T(8,128)(2,1)}), bf16[384,4096]{1,0:T(8,128)(2,1)}) %all-reduce.2.cloned.1.call-update) | async-done | bytes 3145744 | tf_op jit(solution)/shard_map/psum | solution.py:87
  192.5 5.7 %fusion.5 = bf16[384,512]{1,0:T(8,128)(2,1)} fusion(bf16[4096,512]{1,0:T(8,128)(2,1)} %param.31, bf16[384,4096]{1,0:T(8,128)(2,1)} %all-reduce.2.cloned.1.call-done), kind=kOutput, calls=%fused_computation.14 | convolution fusion | flops 1617100800 | bytes 7733248 | tf_op jit(solution)/shard_map/dot_general | solution.py:90
  198.2 0.0 reduce-scatter.5.cloned.1.call-update
  198.2 9.8 %bitcast_add_fusion = f32[96,4,4096]{0,2,1:T(8,128)} fusion(f32[96,4,64,64]{0,3,2,1:T(8,128)} %get-tuple-element.4, f32[96,4,4096]{0,2,1:T(8,128)} %copy.22, f32[96,4]{0,1:T(4,128)S(1)} %fusion.12), kind=kLoop, calls=%fused_computation | loop fusion | flops 3145728 | bytes 18875904 | tf_op jit(solution)/shard_map/add | solution.py:66
  208.0 0.0 copy-start.4
  208.0 0.0 copy-start.1
  208.0 9.6 %copy.27 = f32[96,4,4096]{2,1,0:T(4,128)} copy(f32[96,4,4096]{0,2,1:T(8,128)} %bitcast_add_fusion) | data formatting | bytes 12582912
  217.6 6.4 %reduce-scatter.5.cloned.1.call-done = bf16[96,512]{1,0:T(8,128)(2,1)} async-done(((bf16[384,512]{1,0:T(8,128)(2,1)}), bf16[96,512]{1,0:T(8,128)(2,1)}) %reduce-scatter.5.cloned.1.call-update) | async-done | bytes 98320 | tf_op jit(solution)/shard_map/reduce_scatter | solution.py:89
  224.0 0.0 copy-done.4
  224.0 1.6 add_convert_fusion
  225.6 0.0 copy-done.1
  (8 shorter events, 0.1 us)
Async XLA Ops:
  7.2 45.8 %copy-start = (bf16[256,4096]{1,0:T(8,128)(2,1)S(1)}, bf16[256,4096]{1,0:T(8,128)(2,1)}, u32[]{:S(2)}) copy-start(bf16[256,4096]{1,0:T(8,128)(2,1)} %param.28) | copy-start | bytes 6291460
  7.2 76.6 %reduce-scatter.3.cloned.1.call-start = ((), (), s32[]{:S(2)}) async-start(), calls=%async_computation.2 | async-start | bytes 884736 | tf_op jit(solution)/shard_map/reduce_scatter | solution.py:78
  23.9 3.0 %copy-start.6 = (bf16[4096,256]{1,0:T(8,128)(2,1)S(1)}, bf16[4096,256]{1,0:T(8,128)(2,1)}, u32[]{:S(2)}) copy-start(bf16[4096,256]{1,0:T(8,128)(2,1)} %param.21) | copy-start | bytes 6291460
  23.9 3.0 %copy-start.9 = (f32[4096]{0:T(1024)S(1)}, f32[4096]{0:T(1024)}, u32[]{:S(2)}) copy-start(f32[4096]{0:T(1024)} %param.26) | copy-start | bytes 49156
  26.9 1.6 copy-start.7
  28.5 1.6 copy-start.8
  31.1 10.4 %copy-start.10 = (f32[4]{0:T(128)S(1)}, f32[4]{0:T(128)}, u32[]{:S(2)}) copy-start(f32[4]{0:T(128)} %param.25) | copy-start | bytes 52
  42.8 5.8 %copy-start.2 = (f32[96,4,4096]{0,2,1:T(8,128)S(1)}, f32[96,4,4096]{0,2,1:T(8,128)}, u32[]{:S(2)}) copy-start(f32[96,4,4096]{0,2,1:T(8,128)} %copy.22) | copy-start | bytes 18874372
  48.6 4.2 %copy-start.5 = (f32[64]{0:T(128)S(1)}, f32[64]{0:T(128)}, u32[]{:S(2)}) copy-start(f32[64]{0:T(128)} %param.27) | copy-start | bytes 772
  52.8 31.0 %copy-start.3 = (bf16[96,512]{1,0:T(8,128)(2,1)S(1)}, bf16[96,512]{1,0:T(8,128)(2,1)}, u32[]{:S(2)}) copy-start(bf16[96,512]{1,0:T(8,128)(2,1)} %param.16) | copy-start | bytes 294916
  54.4 138.1 %all-reduce.2.cloned.1.call-start = ((), (), s32[]{:S(2)}) async-start(), calls=%async_computation.3 | async-start | bytes 6291456 | tf_op jit(solution)/shard_map/psum | solution.py:87
  115.1 108.9 %reduce-scatter.5.cloned.1.call-start = ((), (), s32[]{:S(2)}) async-start(), calls=%async_computation.4 | async-start | bytes 491520 | tf_op jit(solution)/shard_map/reduce_scatter | solution.py:89
  208.0 16.0 %copy-start.4 = (bf16[96,512]{1,0:T(8,128)(2,1)S(1)}, bf16[96,512]{1,0:T(8,128)(2,1)}, u32[]{:S(2)}) copy-start(bf16[96,512]{1,0:T(8,128)(2,1)} %reduce-scatter.3.cloned.1.call-done) | copy-start | bytes 294916
  208.0 17.6 %copy-start.1 = (bf16[256,4096]{1,0:T(8,128)(2,1)S(1)}, bf16[256,4096]{1,0:T(8,128)(2,1)}, u32[]{:S(2)}) copy-start(bf16[256,4096]{1,0:T(8,128)(2,1)} %param.28) | copy-start | bytes 6291460
Sparse Core Ops, SparseCore 0:
  54.5 29.2 reduce-scatter.2
  115.2 77.2 all-reduce.1
  198.3 25.6 reduce-scatter.4
where the time goes:
time: 235 us; the launch traced here: 232 us
  waiting for transfers between devices  112 us (48%)
  blocking collectives  39.5 us (17%)
  other arithmetic  23.9 us (10%)
  local copies, waits for them, and re-layouts  21.4 us (9%)
  matrix products  20.9 us (9%)
  between operations  13.9 us (6%)
    psum x1, waiting for transfers between devices, local(): up_full = lax.psum(up_part.astype(jnp.bfloat16), 'tp').astype(jnp.float32)  77.2 us
    reduce_scatter x1, waiting for transfers between devices, local(): lax.psum_scatter(partial_value.astype(jnp.bfloat16), 'tp', scatter_dimens...  28.6 us
    unnamed x24, local copies, waits for them, and re-layouts  20.6 us
    all_gather x1, blocking collectives, local(): full_rows = lax.all_gather(tokens, 'tp', axis=1, tiled=True)  15.9 us
    psum x1, blocking collectives, local(): squares = lax.psum(jnp.sum(resid * resid, axis=-1), 'tp')  13.2 us
    all_gather x1, blocking collectives, local(): lax.all_gather(ffn_in, 'kv', axis=0, tiled=True)  10.4 us
    add x1, other arithmetic, local(): matrix = matrix + key_proj[:, :, :, None] * delta[:, :, None, :]  9.81 us
    reduce_scatter x1, waiting for transfers between devices, local(): lax.psum_scatter(jnp.dot(hidden, w_down, preferred_element_type=jnp.float...  6.4 us
  transfers between devices with their start and end apart: 3, of which 3 were waited for; matrix products, arithmetic and copies ran while one was open for 9% of the time, Pallas kernels for 0%

commit v1 on v0

--- a/solution.py
+++ b/solution.py
@@ -1,9 +1,12 @@
+import functools
+
 import jax
 import jax.numpy as jnp
 from jax import lax
+from jax.experimental import pallas as pl
+from jax.experimental.pallas import tpu as pltpu
 from jax.sharding import PartitionSpec as P
 
-D = 4096
 HEAD_DIM = 64
 
 
@@ -14,7 +17,323 @@
     return vector * lax.rsqrt(jnp.sum(vector * vector, axis=-1, keepdims=True) + EPS)
 
 
+MESH = pl.DeviceIdType.MESH
+VMEM = pltpu.VMEM
+CORES = 2
+
+
+def remote(src, dst, send, recv, where):
+    return pltpu.make_async_remote_copy(
+        src_ref=src, dst_ref=dst, send_sem=send, recv_sem=recv, device_id=where, device_id_type=MESH
+    )
+
+
+def place(chips):
+    me = lax.axis_index("tp")
+    return lax.div(me, CORES), lax.rem(me, CORES)
+
+
+def columns(block, width):
+    return pl.ds(pl.multiple_of(block * width, 128), width)
+
+
+def gather_kernel(chips, x_ref, o_ref, own_sem, send, recv, pass_send, pass_recv):
+    chip, core = place(chips)
+    width = x_ref.shape[1]
+    partner = {"tp": chip * CORES + 1 - core}
+
+    def peer(step):
+        return {"tp": lax.rem(chip + step, chips) * CORES + core}
+
+    barrier = pltpu.get_barrier_semaphore()
+    pl.semaphore_signal(barrier, inc=1, device_id=partner, device_id_type=MESH)
+    for step in range(1, chips):
+        pl.semaphore_signal(barrier, inc=1, device_id=peer(step), device_id_type=MESH)
+    pl.semaphore_wait(barrier, chips)
+
+    mine = columns(chip * CORES + core, width)
+    copies = []
+    for step in range(1, chips):
+        copies.append(remote(x_ref, o_ref.at[:, mine], send.at[step], recv.at[step], peer(step)))
+        copies[-1].start()
+    near = remote(x_ref, o_ref.at[:, mine], send.at[0], recv.at[0], partner)
+    near.start()
+    keep = pltpu.make_async_copy(x_ref, o_ref.at[:, mine], own_sem)
+    keep.start()
+    passed = []
+    for step in range(1, chips):
+        copies[step - 1].wait_recv()
+        block = lax.rem(chip + chips - step, chips) * CORES + core
+        there = o_ref.at[:, columns(block, width)]
+        passed.append(remote(there, there, pass_send.at[step], pass_recv.at[step], partner))
+        passed[-1].start()
+    near.wait()
+    keep.wait()
+    for copy in passed:
+        copy.wait()
+    for copy in copies:
+        copy.wait_send()
+
+
+def gather_tp(tokens, chips):
+    rows, width = tokens.shape
+    return pl.pallas_call(
+        functools.partial(gather_kernel, chips),
+        out_shape=jax.ShapeDtypeStruct((rows, width * chips * CORES), tokens.dtype),
+        in_specs=[pl.BlockSpec(memory_space=VMEM)],
+        out_specs=pl.BlockSpec(memory_space=VMEM),
+        scratch_shapes=[pltpu.SemaphoreType.DMA] + [pltpu.SemaphoreType.DMA((chips,))] * 4,
+        compiler_params=pltpu.CompilerParams(collective_id=0, has_side_effects=True),
+        name="gather_tp",
+    )(tokens)
+
+
+def mixer_kernel(
+    chips, groups, part_ref, tok_ref, gain_ref, up_ref, down_hbm, o_ref,
+    down_ref, pair_in, pair_sum, chip_in, resid_ref, y_ref, sq_ref,
+    up_out, up_in, up_sum, up_far, up_acc, h_ref, acc_ref, d_out, d_in,
+    load_sem, s_pair, r_pair, s_chip, r_chip, s_y, r_y, s_sq, r_sq,
+    s_up, r_up, s_far, r_far, s_h, r_h, s_pass, r_pass, s_d, r_d,
+):
+    chip, core = place(chips)
+    me = chip * CORES + core
+    group = lax.axis_index("kv")
+    ranks = chips * CORES
+    rows, width = tok_ref.shape
+    hid = up_ref.shape[1] // ranks
+    partner = {"tp": chip * CORES + 1 - core}
+    f32, bf16 = jnp.float32, jnp.bfloat16
+
+    def ahead(step):
+        return lax.rem(chip + step, chips)
+
+    def behind(step):
+        return lax.rem(chip + chips - step, chips)
+
+    def peer(step):
+        return {"tp": ahead(step) * CORES + core}
+
+    def rank_peer(step):
+        return {"tp": lax.rem(me + step, ranks)}
+
+    def group_peer(step):
+        return {"kv": lax.rem(group + step, groups)}
+
+    barrier = pltpu.get_barrier_semaphore()
+    for step in range(1, ranks):
+        pl.semaphore_signal(barrier, inc=1, device_id=rank_peer(step), device_id_type=MESH)
+    for step in range(1, groups):
+        pl.semaphore_signal(barrier, inc=1, device_id=group_peer(step), device_id_type=MESH)
+    load = pltpu.make_async_copy(down_hbm, down_ref, load_sem)
+    load.start()
+    pl.semaphore_wait(barrier, ranks + groups - 2)
+
+    order = list(range(1, chips)) + [0]
+    pair = {}
+    for step in order:
+        there = part_ref.at[:, columns(ahead(step) * CORES + 1 - core, width)]
+        pair[step] = remote(there, pair_in.at[step], s_pair.at[step], r_pair.at[step], partner)
+        pair[step].start()
+    far = {}
+    for step in order:
+        pair[step].wait_recv()
+        both = part_ref[:, columns(ahead(step) * CORES + core, width)].astype(f32) + pair_in[
+            step
+        ].astype(f32)
+        if step:
+            pair_sum[step] = both.astype(bf16)
+            far[step] = remote(
+                pair_sum.at[step], chip_in.at[step], s_chip.at[step], r_chip.at[step], peer(step)
+            )
+            far[step].start()
+    resid = tok_ref[...].astype(f32) + both
+    for step in range(1, chips):
+        far[step].wait_recv()
+        resid = resid + chip_in[step].astype(f32)
+    resid_ref[...] = resid
+    y_ref[0] = (resid * gain_ref[...]).astype(bf16)
+    spread = {}
+    for step in range(1, groups):
+        spread[step] = remote(
+            y_ref.at[0], y_ref.at[step], s_y.at[step], r_y.at[step], group_peer(step)
+        )
+        spread[step].start()
+    sq_ref[0] = lax.dot_general(
+        jnp.ones((8, width), f32),
+        resid * resid,
+        (((1,), (1,)), ((), ())),
+        precision=lax.Precision.HIGHEST,
+        preferred_element_type=f32,
+    )
+    squares = {}
+    for step in range(1, ranks):
+        squares[step] = remote(
+            sq_ref.at[0], sq_ref.at[step], s_sq.at[step], r_sq.at[step], rank_peer(step)
+        )
+        squares[step].start()
+    for step in range(1, groups):
+        spread[step].wait_recv()
+
+    all_rows = groups * rows
+
+    def up_block(block):
+        return jnp.dot(
+            y_ref[...].reshape(all_rows, width),
+            up_ref[:, columns(block, hid)],
+            preferred_element_type=f32,
+        )
+
+    def up_pair(step):
+        return remote(up_out.at[step], up_in.at[step], s_up.at[step], r_up.at[step], partner)
+
+    def up_chip(step):
+        return remote(up_sum.at[step], up_far.at[step], s_far.at[step], r_far.at[step], peer(step))
+
+    @pl.loop(0, chips)
+    def _(index):
+        step = lax.rem(index + 1, chips)
+        up_out[step] = up_block(ahead(step) * CORES + 1 - core).astype(bf16)
+        up_pair(step).start()
+
+    @pl.loop(1, chips)
+    def _(step):
+        both = up_block(ahead(step) * CORES + core)
+        up_pair(step).wait_recv()
+        up_sum[step] = (both + up_in[step].astype(f32)).astype(bf16)
+        up_chip(step).start()
+
+    up_acc[...] = up_block(me)
+    up_pair(0).wait_recv()
+    up_acc[...] += up_in[0].astype(f32)
+
+    @pl.loop(1, chips)
+    def _(step):
+        up_chip(step).wait_recv()
+        up_acc[...] += up_far[step].astype(f32)
+
+    h_ref[0] = jnp.square(jnp.maximum(up_acc[...], 0.0)).astype(bf16)
+
+    def h_chip(step):
+        return remote(h_ref.at[0], h_ref.at[step], s_h.at[step], r_h.at[step], peer(step))
+
+    def h_pass(step):
+        return remote(
+            h_ref.at[step], h_ref.at[chips + step], s_pass.at[step], r_pass.at[step], partner
+        )
+
+    @pl.loop(1, chips)
+    def _(step):
+        h_chip(step).start()
+
+    h_pass(0).start()
+    load.wait()
+
+    def down_block(slot, block):
+        return jnp.dot(
+            h_ref[slot],
+            down_ref[pl.ds(pl.multiple_of(block * hid, 128), hid), :],
+            preferred_element_type=f32,
+        )
+
+    acc_ref[...] = down_block(0, me)
+    h_pass(0).wait_recv()
+    acc_ref[...] += down_block(chips, chip * CORES + 1 - core)
+
+    @pl.loop(1, chips)
+    def _(step):
+        h_chip(step).wait_recv()
+        h_pass(step).start()
+        acc_ref[...] += down_block(step, behind(step) * CORES + core)
+        h_pass(step).wait_recv()
+        acc_ref[...] += down_block(chips + step, behind(step) * CORES + 1 - core)
+
+    back = {}
+    for step in range(1, groups):
+        d_out[step] = acc_ref[step * rows : (step + 1) * rows, :].astype(bf16)
+        back[step] = remote(
+            d_out.at[step], d_in.at[step], s_d.at[step], r_d.at[step], group_peer(groups - step)
+        )
+        back[step].start()
+    for step in range(1, ranks):
+        squares[step].wait_recv()
+    total = sq_ref[0]
+    for step in range(1, ranks):
+        total = total + sq_ref[step]
+    spots = lax.dot_general(
+        total,
+        jnp.full((8, width), 0.125, f32),
+        (((0,), (0,)), ((), ())),
+        precision=lax.Precision.HIGHEST,
+        preferred_element_type=f32,
+    )
+    scale = lax.rsqrt(spots * (1.0 / (width * ranks)) + EPS)
+    mixed = acc_ref[0:rows, :]
+    for step in range(1, groups):
+        back[step].wait_recv()
+        mixed = mixed + d_in[step].astype(f32)
+    o_ref[...] = (resid_ref[...] + scale * scale * mixed).astype(bf16)
+
+    for copies in (pair, far, spread, squares, back):
+        for copy in copies.values():
+            copy.wait_send()
+    h_pass(0).wait_send()
+    up_pair(0).wait_send()
+
+    @pl.loop(1, chips)
+    def _(step):
+        up_pair(step).wait_send()
+        up_chip(step).wait_send()
+        h_chip(step).wait_send()
+        h_pass(step).wait_send()
+
+
+def channel_mixer(partial_value, tokens, gain_share, w_up, w_down, chips, groups):
+    rows, width = tokens.shape
+    ranks = chips * CORES
+    hid = w_up.shape[1] // ranks
+    all_rows = groups * rows
+    bf16, f32 = jnp.bfloat16, jnp.float32
+    dma = pltpu.SemaphoreType.DMA
+    spec = pl.BlockSpec(memory_space=VMEM)
+    return pl.pallas_call(
+        functools.partial(mixer_kernel, chips, groups),
+        out_shape=jax.ShapeDtypeStruct((rows, width), bf16),
+        in_specs=[spec] * 4 + [pl.BlockSpec(memory_space=pl.ANY)],
+        out_specs=spec,
+        scratch_shapes=[
+            VMEM(w_down.shape, bf16),
+            VMEM((chips, rows, width), bf16),
+            VMEM((chips, rows, width), bf16),
+            VMEM((chips, rows, width), bf16),
+            VMEM((rows, width), f32),
+            VMEM((groups, rows, width), bf16),
+            VMEM((ranks, 8, rows), f32),
+            VMEM((chips, all_rows, hid), bf16),
+            VMEM((chips, all_rows, hid), bf16),
+            VMEM((chips, all_rows, hid), bf16),
+            VMEM((chips, all_rows, hid), bf16),
+            VMEM((all_rows, hid), f32),
+            VMEM((ranks, all_rows, hid), bf16),
+            VMEM((all_rows, width), f32),
+            VMEM((groups, rows, width), bf16),
+            VMEM((groups, rows, width), bf16),
+            dma,
+        ]
+        + [dma((chips,))] * 4
+        + [dma((groups,))] * 2
+        + [dma((ranks,))] * 2
+        + [dma((chips,))] * 8
+        + [dma((groups,))] * 2,
+        compiler_params=pltpu.CompilerParams(
+            collective_id=1, has_side_effects=True, vmem_limit_bytes=48 * 1024 * 1024
+        ),
+        name="channel_mixer",
+    )(partial_value, tokens, gain_share, w_up, w_down)
+
+
 def local(
+    chips,
+    groups,
     tokens,
     state,
     w_query,
@@ -35,7 +354,7 @@
     rows = tokens.shape[0]
     width_share = tokens.shape[1]
     head_count = w_query.shape[1] // HEAD_DIM
-    full_rows = lax.all_gather(tokens, "tp", axis=1, tiled=True)
+    full_rows = gather_tp(tokens, chips)
     full_f = full_rows.astype(jnp.float32)
     normed = (
         full_f * lax.rsqrt(jnp.mean(full_f * full_f, axis=-1, keepdims=True) + EPS) * mix_gain
@@ -75,24 +394,15 @@
     partial_value = jnp.dot(head_out, w_out, preferred_element_type=jnp.float32)
     feature_start = lax.axis_index("tp") * width_share
     gain_share = lax.dynamic_slice_in_dim(ffn_gain, feature_start, width_share, 0)
-    resid = tokens.astype(jnp.float32) + lax.psum_scatter(
-        partial_value.astype(jnp.bfloat16), "tp", scatter_dimension=1, tiled=True
-    ).astype(jnp.float32)
-    squares = lax.psum(jnp.sum(resid * resid, axis=-1), "tp")
-    scale = lax.rsqrt(squares[:, None] / D + EPS)
-    ffn_in = (resid * scale * gain_share).astype(jnp.bfloat16)
-    up_part = jnp.dot(
-        lax.all_gather(ffn_in, "kv", axis=0, tiled=True), w_up, preferred_element_type=jnp.float32
-    )
-    up_full = lax.psum(up_part.astype(jnp.bfloat16), "tp").astype(jnp.float32)
-    hidden = jnp.square(jax.nn.relu(up_full)).astype(jnp.bfloat16)
-    down = lax.psum_scatter(
-        jnp.dot(hidden, w_down, preferred_element_type=jnp.float32).astype(jnp.bfloat16),
-        "kv",
-        scatter_dimension=0,
-        tiled=True,
-    ).astype(jnp.float32)
-    mixed = (resid + down).astype(jnp.bfloat16)
+    mixed = channel_mixer(
+        partial_value.astype(jnp.bfloat16),
+        tokens,
+        gain_share[None, :],
+        w_up,
+        w_down,
+        chips,
+        groups,
+    )
     return (mixed, matrix.reshape(rows, head_count, HEAD_DIM * HEAD_DIM))
 
 
@@ -116,4 +426,5 @@
         P("kv", "tp"),
     )
     out_specs = (P("kv", "tp"), P("kv", "tp", None))
-    return jax.shard_map(local, mesh=mesh, in_specs=in_specs, out_specs=out_specs, check_vma=False)
+    body = functools.partial(local, mesh.shape["tp"] // CORES, mesh.shape["kv"])
+    return jax.shard_map(body, mesh=mesh, in_specs=in_specs, out_specs=out_specs, check_vma=False)

time: 235 us -> 173 us (0.74); the launches traced: 232 us -> 173 us
  Pallas kernels: 0 us -> 119 us
  waiting for transfers between devices: 112 us -> 0 us
  blocking collectives: 39.5 us -> 0 us
  matrix products: 20.9 us -> 7.42 us
  between operations: 13.9 us -> 0.83 us
  local copies, waits for them, and re-layouts: 21.4 us -> 23.9 us
    pallas_call x0 -> x2, Pallas kernels: none -> 119 us  [the longest x1 104 us: channel_mixer(): pl.pallas_call(functools.partial(mixer_kernel, chips, groups), out_shape=...]
    psum x1 -> x0, waiting for transfers between devices: 77.2 us -> none  [local(): up_full = lax.psum(up_part.astype(jnp.bfloat16), 'tp').astype(jnp.float32)]
    reduce_scatter x2 -> x0, waiting for transfers between devices: 35 us -> none  [the longest x1 28.6 us: local(): lax.psum_scatter(partial_value.astype(jnp.bfloat16), 'tp', scatter_dimens...]
    all_gather x2 -> x0, blocking collectives: 26.2 us -> none  [the longest x1 15.9 us: local(): full_rows = lax.all_gather(tokens, 'tp', axis=1, tiled=True)]
    psum x1 -> x0, blocking collectives: 13.2 us -> none  [local(): squares = lax.psum(jnp.sum(resid * resid, axis=-1), 'tp')]
    dot_general x2 -> x0, matrix products: 11.3 us -> none  [the longest x1 5.68 us: local(): jnp.dot(hidden, w_down, preferred_element_type=jnp.float32)]
    convert_element_type x2 -> x0, other arithmetic: 2.55 us -> none  [the longest x1 1.57 us: local(): mixed = (resid + down).astype(jnp.bfloat16)]
    unnamed x24 -> x25, local copies, waits for them, and re-layouts: 20.6 us -> 23.2 us
  transfers between devices with their start and end apart: 3 -> 0, of which waited for: 3 -> 0; matrix products, arithmetic and copies ran while one was open for 9% -> 0% of each run, Pallas kernels for 0% -> 0%
where the time goes in v1:
time: 173 us
  Pallas kernels  119 us (69%)
  local copies, waits for them, and re-layouts  23.9 us (14%)
  other arithmetic  21.6 us (12%)
  matrix products  7.42 us (4%)
    pallas_call x1, Pallas kernels, channel_mixer(): pl.pallas_call(functools.partial(mixer_kernel, chips, groups), out_shape=...  104 us
    unnamed x25, local copies, waits for them, and re-layouts  23.2 us
    pallas_call x1, Pallas kernels, gather_tp(): pl.pallas_call(functools.partial(gather_kernel, chips), out_shape=jax.Sha...  14.8 us
    add x1, other arithmetic, local(): matrix = matrix + key_proj[:, :, :, None] * delta[:, :, None, :]  9.83 us
    dot_general x1, other arithmetic, local(): jnp.einsum('bhk,bhkv->bhv', key_proj, matrix, precision=lax.Precision.HIG...  4.99 us
    mul x1, other arithmetic, local(): matrix = matrix + key_proj[:, :, :, None] * delta[:, :, None, :]  4.25 us

profile of v1, /device:TPU:24, one launch (start us, length us, event | category | flops | bytes accessed | tf_op | source)
XLA Modules:
  0.0 172.5 jit_solution(15465481711471054285)
XLA Ops:
  0.6 0.0 copy-start
  0.6 0.0 copy-start.10
  0.7 0.8 neg.14
  1.5 0.8 dynamic_slice.11
  2.2 14.8 %gather_tp.1 = bf16[96,4096]{1,0:T(8,128)(2,1)} custom-call(bf16[96,512]{1,0:T(8,128)(2,1)} %tok_ref.1), custom_call_target="tpu_custom_call" | custom-call | tf_op jit(solution)/shard_map/gather_tp/pallas_call | solution.py:80
  17.0 0.0 copy-start.4
  17.0 0.0 copy-start.6
  17.0 1.5 fusion
  18.6 1.6 fusion.9
  20.1 0.0 copy-done.10
  20.1 0.0 copy-done.4
  20.2 0.0 copy-start.7
  20.2 1.4 fusion.5
  21.5 0.0 copy-done.6
  21.5 1.0 fusion.17
  22.5 0.0 copy-start.8
  22.6 0.0 copy-done.7
  22.6 1.0 fusion.14
  23.5 0.0 copy-start.9
  23.6 0.6 copy-done.8
  24.1 1.0 multiply_reduce_fusion.3
  25.1 0.2 copy-done.9
  25.3 1.0 multiply_reduce_fusion.4
  26.4 9.2 %copy.22 = f32[96,4,4096]{0,2,1:T(8,128)} copy(f32[96,4,4096]{2,1,0:T(4,128)} %param.17) | data formatting | bytes 12582912 | tf_op args[1]
  35.5 0.0 copy-start.3
  35.5 5.0 %multiply_reduce_fusion.1 = f32[96,4,64]{0,2,1:T(8,128)S(1)} fusion(f32[96,4,64,64]{0,3,2,1:T(8,128)} %bitcast.20, f32[96,4,64]{0,2,1:T(8,128)S(1)} %broadcast_multiply_fusion.1, f32[96,4]{0,1:T(4,128)S(1)} %fusion.9), kind=kLoop, calls=%fused_computation.2 | loop fusion | flops 4694016 | bytes 6489600 | tf_op jit(solution)/shard_map/bhk,bhkv->bhv/dot_general | solution.py:383
  40.6 0.7 copy-done.3
  41.3 4.2 %broadcast_multiply_fusion = (f32[96,4,64,64]{0,3,2,1:T(8,128)}, f32[96,4,64]{0,2,1:T(8,128)S(1)}) fusion(f32[96,4,64]{0,2,1:T(8,128)S(1)} %get-tuple-element.10, f32[96,4,64]{0,2,1:T(8,128)S(1)} %broadcast_multiply_fusion.1, f32[96,4,64,64]{0,3,2,1:T(8,128)S(1)} %bitcast.21, f32[96,4]{0,1:T(4,128)S(1)} %fusion.9, f32[96,4,64]{0,2,1:T(8,128)S(1)} %get-tuple-element.11), kind=kLoop, calls=%fused_computation.4 | loop fusion | flops 7839744 | bytes 12977664 | tf_op jit(solution)/shard_map/mul | solution.py:385
  45.6 9.8 %bitcast_add_fusion = f32[96,4,4096]{0,2,1:T(8,128)} fusion(f32[96,4,64,64]{0,3,2,1:T(8,128)} %get-tuple-element.4, f32[96,4,4096]{0,2,1:T(8,128)} %copy.22, f32[96,4]{0,1:T(4,128)S(1)} %fusion.9), kind=kLoop, calls=%fused_computation | loop fusion | flops 3145728 | bytes 18875904 | tf_op jit(solution)/shard_map/add | solution.py:385
  55.4 0.0 copy-start.5
  55.4 9.4 %copy.27 = f32[96,4,4096]{2,1,0:T(4,128)} copy(f32[96,4,4096]{0,2,1:T(8,128)} %bitcast_add_fusion) | data formatting | bytes 12582912
  64.8 0.0 copy-start.2
  64.8 0.0 copy-done.5
  64.9 0.1 multiply_convert_fusion
  64.9 0.0 copy-done
  65.0 0.5 convolution_convert_fusion.part_ref
  65.5 0.2 copy-done.2
  65.7 0.0 copy-start.1
  65.7 2.2 %copy-done.1 = bf16[512,4096]{1,0:T(8,128)(2,1)S(1)} copy-done((bf16[512,4096]{1,0:T(8,128)(2,1)S(1)}, bf16[512,4096]{1,0:T(8,128)(2,1)}, u32[]{:S(2)}) %copy-start.1) | copy-done | bytes 4194328
  67.9 104.0 %channel_mixer.1 = bf16[96,512]{1,0:T(8,128)(2,1)S(1)} custom-call(bf16[96,4096]{1,0:T(8,128)(2,1)S(1)} %convolution_convert_fusion.part_ref, bf16[96,512]{1,0:T(8,128)(2,1)S(1)} %copy-done.2, f32[1,512]{1,0:T(1,128)S(1)} %bitcast.19, bf16[512,4096]{1,0:T(8,128)(2,1)S(1)} %copy-done.1, bf16[4096,512]{1,0:T(8,128)(2,1)} %down_hbm.1), custom_call_target="tpu_custom_call" | custom-call | tf_op jit(solution)/shard_map/channel_mixer/pallas_call | solution.py:298
  171.9 0.6 copy.45
  (7 shorter events, 0.1 us)
Async XLA Ops:
  0.6 64.3 %copy-start = (bf16[256,4096]{1,0:T(8,128)(2,1)S(1)}, bf16[256,4096]{1,0:T(8,128)(2,1)}, u32[]{:S(2)}) copy-start(bf16[256,4096]{1,0:T(8,128)(2,1)} %param.28) | copy-start | bytes 6291460
  0.6 19.5 %copy-start.10 = (f32[4096]{0:T(1024)S(1)}, f32[4096]{0:T(1024)}, u32[]{:S(2)}) copy-start(f32[4096]{0:T(1024)} %param.26) | copy-start | bytes 49156
  17.0 3.2 %copy-start.4 = (bf16[96,4096]{1,0:T(8,128)(2,1)S(1)}, bf16[96,4096]{1,0:T(8,128)(2,1)}, u32[]{:S(2)}) copy-start(bf16[96,4096]{1,0:T(8,128)(2,1)} %gather_tp.1) | copy-start | bytes 2359300
  17.0 4.5 %copy-start.6 = (bf16[4096,256]{1,0:T(8,128)(2,1)S(1)}, bf16[4096,256]{1,0:T(8,128)(2,1)}, u32[]{:S(2)}) copy-start(bf16[4096,256]{1,0:T(8,128)(2,1)} %param.20) | copy-start | bytes 6291460
  20.2 2.4 %copy-start.7 = (bf16[4096,256]{1,0:T(8,128)(2,1)S(1)}, bf16[4096,256]{1,0:T(8,128)(2,1)}, u32[]{:S(2)}) copy-start(bf16[4096,256]{1,0:T(8,128)(2,1)} %param.21) | copy-start | bytes 6291460
  22.5 1.6 copy-start.8
  23.5 1.7 %copy-start.9 = (bf16[4096,256]{1,0:T(8,128)(2,1)S(1)}, bf16[4096,256]{1,0:T(8,128)(2,1)}, u32[]{:S(2)}) copy-start(bf16[4096,256]{1,0:T(8,128)(2,1)} %param.18) | copy-start | bytes 6291460
  35.5 5.8 %copy-start.3 = (f32[96,4,4096]{0,2,1:T(8,128)S(1)}, f32[96,4,4096]{0,2,1:T(8,128)}, u32[]{:S(2)}) copy-start(f32[96,4,4096]{0,2,1:T(8,128)} %copy.22) | copy-start | bytes 18874372
  55.4 9.5 %copy-start.5 = (f32[64]{0:T(128)S(1)}, f32[64]{0:T(128)}, u32[]{:S(2)}) copy-start(f32[64]{0:T(128)} %param.27) | copy-start | bytes 772
  64.8 0.9 copy-start.2
  65.7 2.2 %copy-start.1 = (bf16[512,4096]{1,0:T(8,128)(2,1)S(1)}, bf16[512,4096]{1,0:T(8,128)(2,1)}, u32[]{:S(2)}) copy-start(bf16[512,4096]{1,0:T(8,128)(2,1)} %up_ref.1) | copy-start | bytes 12582916

commit v2 on v1

--- a/solution.py
+++ b/solution.py
@@ -331,6 +331,117 @@
     )(partial_value, tokens, gain_share, w_up, w_down)
 
 
+def doubled(x):
+    return jnp.concatenate([x, x], axis=-1)
+
+
+def state_kernel(
+    heads, proj_ref, rates_ref, gain_ref, state_ref, new_ref, out_ref,
+    spread_ref, wide_ref, val_ref, row_ref, head_ref,
+):
+    f32, bf16 = jnp.float32, jnp.bfloat16
+    lanes = 2 * HEAD_DIM
+    count = out_ref.shape[0]
+    full = state_ref.shape[2]
+    pack = 8 // heads
+
+    @pl.when(pl.program_id(0) == 0)
+    def _():
+        feature = lax.broadcasted_iota(jnp.int32, spread_ref.shape, 0)
+        lane = lax.broadcasted_iota(jnp.int32, spread_ref.shape, 1)
+        hit = lax.rem(feature, HEAD_DIM) == lax.div(lane, HEAD_DIM)
+        spread_ref[...] = jnp.where(hit, 1.0, 0.0).astype(bf16)
+
+    query = unit_norm(proj_ref[0]) * HEAD_DIM ** (-0.5)
+    key_proj = unit_norm(proj_ref[1])
+    match = jnp.sum(query * key_proj, axis=-1, keepdims=True)
+    both = doubled(jnp.concatenate([key_proj, query], axis=0))
+    high = both.astype(bf16).astype(f32)
+    rest = both - high
+    middle = rest.astype(bf16).astype(f32)
+    low = rest - middle
+    first = lax.broadcasted_iota(jnp.int32, both.shape, 1) < HEAD_DIM
+    parts = jnp.concatenate(
+        [jnp.where(first, high, middle), jnp.where(first, low, 0.0)], axis=-1
+    ).astype(bf16)
+    wide_ref[...] = jnp.dot(parts, spread_ref[...], preferred_element_type=f32)
+    val_ref[...] = doubled(proj_ref[2])
+    row_ref[0] = jnp.broadcast_to(rates_ref[:, 0:1], (count, lanes))
+    row_ref[1] = jnp.broadcast_to(rates_ref[:, 1:2], (count, lanes))
+    row_ref[2] = jnp.broadcast_to(match, (count, lanes))
+
+    @pl.loop(0, count // 8)
+    def _(index):
+        here = pl.ds(pl.multiple_of(index * 8, 8), 8)
+        there = pl.ds(pl.multiple_of(index * 8 + count, 8), 8)
+
+        def state_at(at):
+            return jnp.concatenate(
+                [state_ref[index * pack + i, :, at] for i in range(pack)], axis=0
+            )
+
+        by_key = jnp.zeros((8, lanes), f32)
+        by_query = jnp.zeros((8, lanes), f32)
+        for start in range(0, full, lanes):
+            at = slice(start, start + lanes)
+            now = state_at(at)
+            by_key = by_key + now * wide_ref[here, at]
+            by_query = by_query + now * wide_ref[there, at]
+        by_key = by_key + pltpu.roll(by_key, HEAD_DIM, 1)
+        by_query = by_query + pltpu.roll(by_query, HEAD_DIM, 1)
+        decay = row_ref[0, here, :]
+        delta = (val_ref[here, :] - decay * by_key) * row_ref[1, here, :]
+        head_ref[here, :] = decay * by_query + row_ref[2, here, :] * delta
+        for start in range(0, full, lanes):
+            at = slice(start, start + lanes)
+            new = decay * state_at(at) + wide_ref[here, at] * delta
+            for i in range(pack):
+                new_ref[index * pack + i, :, at] = new[i * heads : (i + 1) * heads]
+
+    head_out = head_ref[:, 0:HEAD_DIM]
+    gate = proj_ref[3]
+    out_ref[...] = (
+        head_out
+        * lax.rsqrt(jnp.mean(head_out * head_out, axis=-1, keepdims=True) + EPS)
+        * gain_ref[...]
+        * (gate * jax.nn.sigmoid(gate))
+    ).astype(bf16)
+
+
+def update_state(proj, rates, out_gain, state):
+    rows, heads, full = state.shape
+    block = rows // 3
+    count = block * heads
+    f32, bf16 = jnp.float32, jnp.bfloat16
+    return pl.pallas_call(
+        functools.partial(state_kernel, heads),
+        grid=(rows // block,),
+        out_shape=(
+            jax.ShapeDtypeStruct(state.shape, f32),
+            jax.ShapeDtypeStruct((rows * heads, HEAD_DIM), bf16),
+        ),
+        in_specs=[
+            pl.BlockSpec((4, count, HEAD_DIM), lambda i: (0, i, 0)),
+            pl.BlockSpec((count, 2), lambda i: (i, 0)),
+            pl.BlockSpec((1, HEAD_DIM), lambda i: (0, 0)),
+            pl.BlockSpec((block, heads, full), lambda i: (i, 0, 0)),
+        ],
+        out_specs=(
+            pl.BlockSpec((block, heads, full), lambda i: (i, 0, 0)),
+            pl.BlockSpec((count, HEAD_DIM), lambda i: (i, 0)),
+        ),
+        scratch_shapes=[
+            VMEM((4 * HEAD_DIM, full), bf16),
+            VMEM((2 * count, full), f32),
+            VMEM((count, 2 * HEAD_DIM), f32),
+            VMEM((3, count, 2 * HEAD_DIM), f32),
+            VMEM((count, 2 * HEAD_DIM), f32),
+        ],
+        compiler_params=pltpu.CompilerParams(vmem_limit_bytes=32 * 1024 * 1024),
+        name="update_state",
+    )(proj, rates, out_gain, state)
+
+
 def local(
     chips,
     groups,
@@ -359,38 +470,21 @@
     normed = (
         full_f * lax.rsqrt(jnp.mean(full_f * full_f, axis=-1, keepdims=True) + EPS) * mix_gain
     ).astype(jnp.bfloat16)
-    query = jnp.dot(normed, w_query, preferred_element_type=jnp.float32).reshape(
-        rows, head_count, HEAD_DIM
-    )
-    key_proj = jnp.dot(normed, w_key, preferred_element_type=jnp.float32).reshape(
-        rows, head_count, HEAD_DIM
-    )
-    value = jnp.dot(normed, w_value, preferred_element_type=jnp.float32).reshape(
-        rows, head_count, HEAD_DIM
-    )
-    gate = jnp.dot(normed, w_gate, preferred_element_type=jnp.float32).reshape(
-        rows, head_count, HEAD_DIM
-    )
-    query = unit_norm(query) * HEAD_DIM ** (-0.5)
-    key_proj = unit_norm(key_proj)
+    proj = jnp.stack(
+        [
+            jnp.dot(normed, w, preferred_element_type=jnp.float32)
+            for w in (w_query, w_key, w_value, w_gate)
+        ]
+    ).reshape(4, rows * head_count, HEAD_DIM)
     head_start = lax.axis_index("tp") * head_count
     decay_cols = lax.dynamic_slice_in_dim(w_decay, head_start, head_count, 1)
     beta_cols = lax.dynamic_slice_in_dim(w_beta, head_start, head_count, 1)
     pre_decay = jnp.dot(normed, decay_cols, preferred_element_type=jnp.float32)
     decay = jnp.exp(-decay_rate * jax.nn.softplus(pre_decay + decay_bias))
     strength = jax.nn.sigmoid(jnp.dot(normed, beta_cols, preferred_element_type=jnp.float32))
-    matrix = state.reshape(rows, head_count, HEAD_DIM, HEAD_DIM) * decay[:, :, None, None]
-    recalled = jnp.einsum("bhk,bhkv->bhv", key_proj, matrix, precision=lax.Precision.HIGHEST)
-    delta = (value - recalled) * strength[:, :, None]
-    matrix = matrix + key_proj[:, :, :, None] * delta[:, :, None, :]
-    head_out = jnp.einsum("bhk,bhkv->bhv", query, matrix, precision=lax.Precision.HIGHEST)
-    head_out = (
-        head_out
-        * lax.rsqrt(jnp.mean(head_out * head_out, axis=-1, keepdims=True) + EPS)
-        * out_gain
-        * jax.nn.silu(gate)
-    )
-    head_out = head_out.reshape(rows, head_count * HEAD_DIM).astype(jnp.bfloat16)
+    rates = jnp.stack([decay, strength], axis=-1).reshape(rows * head_count, 2)
+    new_state, head_out = update_state(proj, rates, out_gain[None, :], state)
+    head_out = head_out.reshape(rows, head_count * HEAD_DIM)
     partial_value = jnp.dot(head_out, w_out, preferred_element_type=jnp.float32)
     feature_start = lax.axis_index("tp") * width_share
     gain_share = lax.dynamic_slice_in_dim(ffn_gain, feature_start, width_share, 0)
@@ -403,7 +497,7 @@
         chips,
         groups,
     )
-    return (mixed, matrix.reshape(rows, head_count, HEAD_DIM * HEAD_DIM))
+    return (mixed, new_state)
 
 
 def solution(mesh):

time: 173 us -> 157 us (0.908)
  other arithmetic: 21.6 us -> 2.38 us
  local copies, waits for them, and re-layouts: 23.9 us -> 9.97 us
  Pallas kernels: 119 us -> 130 us
  matrix products: 7.42 us -> 13.6 us
    unnamed x25 -> x19, local copies, waits for them, and re-layouts: 23.2 us -> 5.65 us
    pallas_call x0 -> x1, Pallas kernels: none -> 10.8 us  [update_state(): pl.pallas_call(functools.partial(state_kernel, heads), grid=(rows // bloc...]
    add x1 -> x0, other arithmetic: 9.83 us -> none  [local(): matrix = matrix + key_proj[:, :, :, None] * delta[:, :, None, :]]
    dot_general x4, matrix products: 3.99 us -> 10 us  [local(): jnp.dot(normed, w, preferred_element_type=jnp.float32)]
    dot_general x1 -> x0, other arithmetic: 4.99 us -> none  [local(): jnp.einsum('bhk,bhkv->bhv', key_proj, matrix, precision=lax.Precision.HIG...]
    mul x3 -> x0, other arithmetic: 4.3 us -> none  [the longest x1 4.25 us: local(): matrix = matrix + key_proj[:, :, :, None] * delta[:, :, None, :]]
    another operation x0 -> x7, local copies, waits for them, and re-layouts: none -> 3.21 us  [the longest x4 2.85 us: local(): jnp.stack([jnp.dot(normed, w, preferred_element_type=jnp.float32) for w i...]
where the time goes in v2:
time: 157 us; the launch traced here: 156 us
  Pallas kernels  130 us (83%)
  matrix products  13.6 us (9%)
  local copies, waits for them, and re-layouts  9.97 us (6%)
  other arithmetic  2.38 us (2%)
    pallas_call x1, Pallas kernels, channel_mixer(): pl.pallas_call(functools.partial(mixer_kernel, chips, groups), out_shape=...  104 us
    pallas_call x1, Pallas kernels, gather_tp(): pl.pallas_call(functools.partial(gather_kernel, chips), out_shape=jax.Sha...  14.9 us
    pallas_call x1, Pallas kernels, update_state(): pl.pallas_call(functools.partial(state_kernel, heads), grid=(rows // bloc...  10.8 us
    dot_general x4, matrix products, local(): jnp.dot(normed, w, preferred_element_type=jnp.float32)  10 us
    unnamed x19, local copies, waits for them, and re-layouts  5.65 us

profile of v2, /device:TPU:24, one launch (start us, length us, event | category | flops | bytes accessed | tf_op | source)
XLA Modules:
  0.0 156.5 jit_solution(7128819204042651830)
XLA Ops:
  0.6 0.0 copy-start
  0.6 0.0 copy-start.6
  0.7 14.9 %gather_tp.1 = bf16[96,4096]{1,0:T(8,128)(2,1)} custom-call(bf16[96,512]{1,0:T(8,128)(2,1)} %tok_ref.1), custom_call_target="tpu_custom_call" | custom-call | tf_op jit(solution)/shard_map/gather_tp/pallas_call | solution.py:80
  15.6 1.4 fusion
  17.0 0.0 copy-done.6
  17.0 0.0 copy-start.5
  17.0 2.4 %fusion.22 = f32[96,256]{1,0:T(8,128)S(1)} fusion(bf16[4096,256]{1,0:T(8,128)(2,1)} %param.18, bf16[96,4096]{1,0:T(8,128)(2,1)} %gather_tp.1, f32[4096]{0:T(1024)S(1)} %copy-done.6, f32[96]{0:T(128)S(1)} %add_rsqrt_fusion), kind=kOutput, calls=%fused_computation.24 | convolution fusion | flops 202899456 | bytes 2998656 | tf_op jit(solution)/shard_map/dot_general | solution.py:475
  19.4 0.1 stack.24
  19.5 0.0 copy-done.5
  19.5 2.1 %fusion.20 = f32[96,256]{1,0:T(8,128)S(1)} fusion(bf16[4096,256]{1,0:T(8,128)(2,1)} %param.19, bf16[96,4096]{1,0:T(8,128)(2,1)S(1)} %copy-done.5, f32[4096]{0:T(1024)S(1)} %copy-done.6, f32[96]{0:T(128)S(1)} %add_rsqrt_fusion), kind=kOutput, calls=%fused_computation.23 | convolution fusion | flops 202899456 | bytes 2998656 | tf_op jit(solution)/shard_map/dot_general | solution.py:475
  21.6 0.1 stack.25
  21.7 2.8 %fusion.18 = f32[96,256]{1,0:T(8,128)} fusion(bf16[4096,256]{1,0:T(8,128)(2,1)} %param.20, bf16[96,4096]{1,0:T(8,128)(2,1)S(1)} %copy-done.5, f32[4096]{0:T(1024)S(1)} %copy-done.6, f32[96]{0:T(128)S(1)} %add_rsqrt_fusion), kind=kOutput, calls=%fused_computation.22 | convolution fusion | flops 202899456 | bytes 2998656 | tf_op jit(solution)/shard_map/dot_general | solution.py:475
  24.5 1.0 stack.26
  25.5 2.8 %fusion.16 = f32[96,256]{1,0:T(8,128)} fusion(bf16[4096,256]{1,0:T(8,128)(2,1)} %param.21, bf16[96,4096]{1,0:T(8,128)(2,1)S(1)} %copy-done.5, f32[4096]{0:T(1024)S(1)} %copy-done.6, f32[96]{0:T(128)S(1)} %add_rsqrt_fusion), kind=kOutput, calls=%fused_computation.21 | convolution fusion | flops 202899456 | bytes 2998656 | tf_op jit(solution)/shard_map/dot_general | solution.py:475
  28.2 0.0 copy-start.7
  28.2 0.0 copy-start.8
  28.2 1.7 %stack.27 = f32[1,384,64]{2,1,0:T(8,128)} reshape(f32[96,256]{1,0:T(8,128)} %fusion.16) | data formatting | bytes 196608 | tf_op jit(solution)/shard_map/stack | solution.py:473
  29.9 1.0 pad_maximum_fusion.proj_ref
  30.9 0.0 copy-done.7
  30.9 0.0 copy-done.8
  30.9 0.0 copy-start.4
  31.0 1.5 fusion.9
  32.5 0.1 copy.24
  32.6 0.1 stack.29
  32.7 1.5 fusion.5
  34.3 0.1 copy.25
  34.4 0.1 stack.30
  34.5 0.1 copy.26.rates_ref
  34.7 0.0 copy-done.4
  34.7 0.0 copy-start.1
  34.7 2.8 %copy-done.1 = f32[96,4,4096]{2,1,0:T(4,128)S(1)} copy-done((f32[96,4,4096]{2,1,0:T(4,128)S(1)}, f32[96,4,4096]{2,1,0:T(4,128)}, u32[]{:S(2)}) %copy-start.1) | copy-done | bytes 6291480
  37.5 10.8 %update_state.1 = (f32[96,4,4096]{2,1,0:T(4,128)}, bf16[384,64]{1,0:T(8,128)(2,1)S(1)}) custom-call(f32[4,384,64]{2,1,0:T(8,128)S(1)} %pad_maximum_fusion.proj_ref, f32[384,2]{1,0:T(8,128)S(1)} %copy.26.rates_ref, f32[1,64]{1,0:T(1,128)S(1)} %bitcast.9, f32[96,4,4096]{2,1,0:T(4,128)S(1)} %copy-done.1), custom_call_target="tpu_custom_call" | custom-call | tf_op jit(solution)/shard_map/update_state/pallas_call | solution.py:416
  48.2 0.0 copy-start.3
  48.2 0.1 reshape.32
  48.4 0.0 copy-done
  48.4 0.5 convolution_convert_fusion.part_ref
  48.8 0.8 dynamic_slice.11
  49.6 0.0 copy-done.3
  49.6 0.0 copy-start.2
  49.6 2.2 %copy-done.2 = bf16[512,4096]{1,0:T(8,128)(2,1)S(1)} copy-done((bf16[512,4096]{1,0:T(8,128)(2,1)S(1)}, bf16[512,4096]{1,0:T(8,128)(2,1)}, u32[]{:S(2)}) %copy-start.2) | copy-done | bytes 4194328
  51.8 104.0 %channel_mixer.1 = bf16[96,512]{1,0:T(8,128)(2,1)S(1)} custom-call(bf16[96,4096]{1,0:T(8,128)(2,1)S(1)} %convolution_convert_fusion.part_ref, bf16[96,512]{1,0:T(8,128)(2,1)S(1)} %copy-done.3, f32[1,512]{1,0:T(1,128)S(1)} %bitcast.8, bf16[512,4096]{1,0:T(8,128)(2,1)S(1)} %copy-done.2, bf16[4096,512]{1,0:T(8,128)(2,1)} %down_hbm.1), custom_call_target="tpu_custom_call" | custom-call | tf_op jit(solution)/shard_map/channel_mixer/pallas_call | solution.py:298
  155.8 0.6 copy.28
  (3 shorter events, 0.0 us)
Async XLA Ops:
  0.6 47.7 %copy-start = (bf16[256,4096]{1,0:T(8,128)(2,1)S(1)}, bf16[256,4096]{1,0:T(8,128)(2,1)}, u32[]{:S(2)}) copy-start(bf16[256,4096]{1,0:T(8,128)(2,1)} %param.28) | copy-start | bytes 6291460
  0.6 16.3 %copy-start.6 = (f32[4096]{0:T(1024)S(1)}, f32[4096]{0:T(1024)}, u32[]{:S(2)}) copy-start(f32[4096]{0:T(1024)} %param.26) | copy-start | bytes 49156
  17.0 2.5 %copy-start.5 = (bf16[96,4096]{1,0:T(8,128)(2,1)S(1)}, bf16[96,4096]{1,0:T(8,128)(2,1)}, u32[]{:S(2)}) copy-start(bf16[96,4096]{1,0:T(8,128)(2,1)} %gather_tp.1) | copy-start | bytes 2359300
  28.2 2.7 %copy-start.7 = (f32[4]{0:T(128)S(1)}, f32[4]{0:T(128)}, u32[]{:S(2)}) copy-start(f32[4]{0:T(128)} %param.24) | copy-start | bytes 52
  28.2 2.7 %copy-start.8 = (f32[4]{0:T(128)S(1)}, f32[4]{0:T(128)}, u32[]{:S(2)}) copy-start(f32[4]{0:T(128)} %param.25) | copy-start | bytes 52
  30.9 3.7 %copy-start.4 = (f32[64]{0:T(128)S(1)}, f32[64]{0:T(128)}, u32[]{:S(2)}) copy-start(f32[64]{0:T(128)} %param.27) | copy-start | bytes 772
  34.7 2.8 %copy-start.1 = (f32[96,4,4096]{2,1,0:T(4,128)S(1)}, f32[96,4,4096]{2,1,0:T(4,128)}, u32[]{:S(2)}) copy-start(f32[96,4,4096]{2,1,0:T(4,128)} %state_ref.1) | copy-start | bytes 18874372
  48.2 1.4 copy-start.3
  49.6 2.2 %copy-start.2 = (bf16[512,4096]{1,0:T(8,128)(2,1)S(1)}, bf16[512,4096]{1,0:T(8,128)(2,1)}, u32[]{:S(2)}) copy-start(bf16[512,4096]{1,0:T(8,128)(2,1)} %up_ref.1) | copy-start | bytes 12582916

commit v3 on v2

--- a/solution.py
+++ b/solution.py
@@ -37,63 +37,126 @@
     return pl.ds(pl.multiple_of(block * width, 128), width)
 
 
-def gather_kernel(chips, x_ref, o_ref, own_sem, send, recv, pass_send, pass_recv):
+def project_kernel(
+    chips, x_ref, gain_ref, decay_ref, beta_ref, wq_hbm, wk_hbm, wv_hbm, wg_hbm,
+    proj_ref, rate_ref, blocks_ref, w_ref, square_ref, load_sem, own_sem,
+    send, recv, pass_send, pass_recv,
+):
+    f32, bf16 = jnp.float32, jnp.bfloat16
     chip, core = place(chips)
+    me = chip * CORES + core
     width = x_ref.shape[1]
+    out_width = wq_hbm.shape[1]
     partner = {"tp": chip * CORES + 1 - core}
 
     def peer(step):
         return {"tp": lax.rem(chip + step, chips) * CORES + core}
+
+    def source(step):
+        return lax.rem(chip + chips - step, chips) * CORES
 
     barrier = pltpu.get_barrier_semaphore()
     pl.semaphore_signal(barrier, inc=1, device_id=partner, device_id_type=MESH)
     for step in range(1, chips):
         pl.semaphore_signal(barrier, inc=1, device_id=peer(step), device_id_type=MESH)
+    loads = []
+    for i, hbm in enumerate((wq_hbm, wk_hbm, wv_hbm, wg_hbm)):
+        there = w_ref.at[:, i * out_width : (i + 1) * out_width]
+        loads.append(pltpu.make_async_copy(hbm, there, load_sem.at[i]))
+        loads[-1].start()
+    keep = pltpu.make_async_copy(x_ref, blocks_ref.at[me], own_sem)
+    keep.start()
+    proj_ref[...] = jnp.zeros_like(proj_ref)
+    rate_ref[...] = jnp.zeros_like(rate_ref)
+    square_ref[...] = jnp.zeros_like(square_ref)
     pl.semaphore_wait(barrier, chips)
 
-    mine = columns(chip * CORES + core, width)
-    copies = []
+    def far(step):
+        return remote(x_ref, blocks_ref.at[me], send.at[step], recv.at[step], peer(step))
+
+    def passed(step):
+        there = blocks_ref.at[source(step) + core]
+        return remote(there, there, pass_send.at[step], pass_recv.at[step], partner)
+
     for step in range(1, chips):
-        copies.append(remote(x_ref, o_ref.at[:, mine], send.at[step], recv.at[step], peer(step)))
-        copies[-1].start()
-    near = remote(x_ref, o_ref.at[:, mine], send.at[0], recv.at[0], partner)
+        far(step).start()
+    near = remote(x_ref, blocks_ref.at[me], send.at[0], recv.at[0], partner)
     near.start()
-    keep = pltpu.make_async_copy(x_ref, o_ref.at[:, mine], own_sem)
-    keep.start()
-    passed = []
-    for step in range(1, chips):
-        copies[step - 1].wait_recv()
-        block = lax.rem(chip + chips - step, chips) * CORES + core
-        there = o_ref.at[:, columns(block, width)]
-        passed.append(remote(there, there, pass_send.at[step], pass_recv.at[step], partner))
-        passed[-1].start()
-    near.wait()
     keep.wait()
-    for copy in passed:
-        copy.wait()
-    for copy in copies:
-        copy.wait_send()
-
-
-def gather_tp(tokens, chips):
+    for load in loads:
+        load.wait()
+
+    def use(block):
+        at = columns(block, width)
+        raw = blocks_ref[block].astype(f32)
+        square_ref[...] += jnp.sum(raw * raw, axis=-1, keepdims=True)
+        scaled = (raw * gain_ref[:, at]).astype(bf16)
+        proj_ref[...] += jnp.dot(scaled, w_ref[at, :], preferred_element_type=f32)
+        rate_ref[0] += jnp.dot(scaled, decay_ref[at, :], preferred_element_type=f32)
+        rate_ref[1] += jnp.dot(scaled, beta_ref[at, :], preferred_element_type=f32)
+
+    use(me)
+    near.wait_recv()
+    use(source(0) + 1 - core)
+
+    @pl.loop(1, chips)
+    def _(step):
+        far(step).wait_recv()
+        passed(step).start()
+        use(source(step) + core)
+
+    @pl.loop(1, chips)
+    def _(step):
+        passed(step).wait_recv()
+        use(source(step) + 1 - core)
+
+    scale = lax.rsqrt(square_ref[...] * (1.0 / (width * chips * CORES)) + EPS)
+    proj_ref[...] = proj_ref[...] * scale
+    rate_ref[0] = rate_ref[0] * scale
+    rate_ref[1] = rate_ref[1] * scale
+    near.wait_send()
+
+    @pl.loop(1, chips)
+    def _(step):
+        far(step).wait_send()
+        passed(step).wait_send()
+
+
+def project(tokens, mix_gain, w_decay, w_beta, weights, chips):
     rows, width = tokens.shape
+    full, out_width = weights[0].shape
+    heads = w_decay.shape[1]
+    dma = pltpu.SemaphoreType.DMA
+    spec = pl.BlockSpec(memory_space=VMEM)
     return pl.pallas_call(
-        functools.partial(gather_kernel, chips),
-        out_shape=jax.ShapeDtypeStruct((rows, width * chips * CORES), tokens.dtype),
-        in_specs=[pl.BlockSpec(memory_space=VMEM)],
-        out_specs=pl.BlockSpec(memory_space=VMEM),
-        scratch_shapes=[pltpu.SemaphoreType.DMA] + [pltpu.SemaphoreType.DMA((chips,))] * 4,
-        compiler_params=pltpu.CompilerParams(collective_id=0, has_side_effects=True),
-        name="gather_tp",
-    )(tokens)
+        functools.partial(project_kernel, chips),
+        out_shape=(
+            jax.ShapeDtypeStruct((rows, 4 * out_width), jnp.float32),
+            jax.ShapeDtypeStruct((2, rows, heads), jnp.float32),
+        ),
+        in_specs=[spec] * 4 + [pl.BlockSpec(memory_space=pl.ANY)] * 4,
+        out_specs=(spec, spec),
+        scratch_shapes=[
+            VMEM((chips * CORES, rows, width), tokens.dtype),
+            VMEM((full, 4 * out_width), jnp.bfloat16),
+            VMEM((rows, 1), jnp.float32),
+            dma((4,)),
+            dma,
+        ]
+        + [dma((chips,))] * 4,
+        compiler_params=pltpu.CompilerParams(
+            collective_id=0, has_side_effects=True, vmem_limit_bytes=40 * 1024 * 1024
+        ),
+        name="project",
+    )(tokens, mix_gain, w_decay, w_beta, *weights)
 
 
 def mixer_kernel(
-    chips, groups, part_ref, tok_ref, gain_ref, up_ref, down_hbm, o_ref,
-    down_ref, pair_in, pair_sum, chip_in, resid_ref, y_ref, sq_ref,
-    up_out, up_in, up_sum, up_far, up_acc, h_ref, acc_ref, d_out, d_in,
-    load_sem, s_pair, r_pair, s_chip, r_chip, s_y, r_y, s_sq, r_sq,
-    s_up, r_up, s_far, r_far, s_h, r_h, s_pass, r_pass, s_d, r_d,
+    chips, groups, part_ref, tok_ref, gain_ref, up_hbm, down_hbm, o_ref,
+    up_ref, down_ref, pair_in, pair_sum, chip_in, resid_ref, y_ref, sq_ref,
+    up_out, up_in, own_ref, sum_out, from_left, from_right, up_acc, h_ref, acc_ref, d_out, d_in,
+    up_load_sem, load_sem, s_pair, r_pair, s_chip, r_chip, s_y, r_y, s_sq, r_sq,
+    s_up, r_up, s_sr, r_sr, s_sl, r_sl, s_gr, r_gr, s_gl, r_gl, s_pass, r_pass, s_d, r_d,
 ):
     chip, core = place(chips)
     me = chip * CORES + core
@@ -107,9 +170,6 @@
     def ahead(step):
         return lax.rem(chip + step, chips)
 
-    def behind(step):
-        return lax.rem(chip + chips - step, chips)
-
     def peer(step):
         return {"tp": ahead(step) * CORES + core}
 
@@ -124,6 +184,8 @@
         pl.semaphore_signal(barrier, inc=1, device_id=rank_peer(step), device_id_type=MESH)
     for step in range(1, groups):
         pl.semaphore_signal(barrier, inc=1, device_id=group_peer(step), device_id_type=MESH)
+    up_load = pltpu.make_async_copy(up_hbm, up_ref, up_load_sem)
+    up_load.start()
     load = pltpu.make_async_copy(down_hbm, down_ref, load_sem)
     load.start()
     pl.semaphore_wait(barrier, ranks + groups - 2)
@@ -174,78 +236,176 @@
     for step in range(1, groups):
         spread[step].wait_recv()
 
-    all_rows = groups * rows
-
-    def up_block(block):
+    half = groups * rows // 2
+    last = chips - 1
+    right = {"tp": lax.rem(me + CORES, ranks)}
+    left = {"tp": lax.rem(me + ranks - CORES, ranks)}
+
+    def span(part):
+        return pl.ds(part * half, half)
+
+    def up_block(part, block):
+        wanted = y_ref[part * groups // 2 : (part + 1) * groups // 2]
         return jnp.dot(
-            y_ref[...].reshape(all_rows, width),
+            wanted.reshape(half, width),
             up_ref[:, columns(block, hid)],
             preferred_element_type=f32,
         )
 
-    def up_pair(step):
-        return remote(up_out.at[step], up_in.at[step], s_up.at[step], r_up.at[step], partner)
-
-    def up_chip(step):
-        return remote(up_sum.at[step], up_far.at[step], s_far.at[step], r_far.at[step], peer(step))
-
-    @pl.loop(0, chips)
-    def _(index):
-        step = lax.rem(index + 1, chips)
-        up_out[step] = up_block(ahead(step) * CORES + 1 - core).astype(bf16)
-        up_pair(step).start()
-
-    @pl.loop(1, chips)
-    def _(step):
-        both = up_block(ahead(step) * CORES + core)
-        up_pair(step).wait_recv()
-        up_sum[step] = (both + up_in[step].astype(f32)).astype(bf16)
-        up_chip(step).start()
-
-    up_acc[...] = up_block(me)
-    up_pair(0).wait_recv()
-    up_acc[...] += up_in[0].astype(f32)
-
-    @pl.loop(1, chips)
-    def _(step):
-        up_chip(step).wait_recv()
-        up_acc[...] += up_far[step].astype(f32)
-
-    h_ref[0] = jnp.square(jnp.maximum(up_acc[...], 0.0)).astype(bf16)
-
-    def h_chip(step):
-        return remote(h_ref.at[0], h_ref.at[step], s_h.at[step], r_h.at[step], peer(step))
-
-    def h_pass(step):
-        return remote(
-            h_ref.at[step], h_ref.at[chips + step], s_pass.at[step], r_pass.at[step], partner
-        )
-
-    @pl.loop(1, chips)
-    def _(step):
-        h_chip(step).start()
-
-    h_pass(0).start()
-    load.wait()
-
-    def down_block(slot, block):
-        return jnp.dot(
-            h_ref[slot],
+    def up_pair(part, t):
+        i = part * chips + t
+        at = span(part)
+        return remote(up_out.at[t, at], up_in.at[t, at], s_up.at[i], r_up.at[i], partner)
+
+    def sum_right(part, t):
+        i = part * chips + t
+        at = span(part)
+        return remote(sum_out.at[t, at], from_left.at[t, at], s_sr.at[i], r_sr.at[i], right)
+
+    def sum_left(part, t):
+        i = part * chips + t
+        at = span(part)
+        return remote(sum_out.at[t, at], from_right.at[t, at], s_sl.at[i], r_sl.at[i], left)
+
+    def block_right(part, t):
+        i = part * chips + t
+        there = h_ref.at[t * CORES + core, span(part)]
+        return remote(there, there, s_gr.at[i], r_gr.at[i], right)
+
+    def block_left(part, t):
+        i = part * chips + t
+        there = h_ref.at[t * CORES + core, span(part)]
+        return remote(there, there, s_gl.at[i], r_gl.at[i], left)
+
+    def block_pass(part, t):
+        i = part * chips + t
+        there = h_ref.at[t * CORES + core, span(part)]
+        return remote(there, there, s_pass.at[i], r_pass.at[i], partner)
+
+    def up(part):
+        at = span(part)
+
+        @pl.loop(0, chips)
+        def _(t):
+            up_out[t, at] = up_block(part, t * CORES + 1 - core).astype(bf16)
+            up_pair(part, t).start()
+
+        @pl.loop(0, chips)
+        def _(t):
+            own = up_block(part, t * CORES + core)
+            up_pair(part, t).wait_recv()
+            own_ref[t, at] = own + up_in[t, at].astype(f32)
+
+    def sum_step(part, step):
+        at = span(part)
+        for t, going, first, more, copy, arrived in (
+            (last - step, chip < last - step, chip == 0, chip > 0, sum_right, from_left),
+            (step, chip > step, chip == last, chip < last, sum_left, from_right),
+        ):
+
+            @pl.when(jnp.logical_and(going, first))
+            def _():
+                sum_out[t, at] = own_ref[t, at].astype(bf16)
+                copy(part, t).start()
+
+            @pl.when(jnp.logical_and(going, more))
+            def _():
+                copy(part, t).wait_recv()
+                sum_out[t, at] = (own_ref[t, at] + arrived[t, at].astype(f32)).astype(bf16)
+                copy(part, t).start()
+
+    def sum_end(part):
+        at = span(part)
+        up_acc[...] = own_ref[chip, at]
+
+        @pl.when(chip > 0)
+        def _():
+            sum_right(part, chip).wait_recv()
+            up_acc[...] += from_left[chip, at].astype(f32)
+
+        @pl.when(chip < last)
+        def _():
+            sum_left(part, chip).wait_recv()
+            up_acc[...] += from_right[chip, at].astype(f32)
+
+        h_ref[me, at] = jnp.square(jnp.maximum(up_acc[...], 0.0)).astype(bf16)
+
+        @pl.when(chip < last)
+        def _():
+            block_right(part, chip).start()
+
+        @pl.when(chip > 0)
+        def _():
+            block_left(part, chip).start()
+
+        block_pass(part, chip).start()
+
+    def down_add(part, block):
+        acc_ref[span(part)] += jnp.dot(
+            h_ref[block, span(part)],
             down_ref[pl.ds(pl.multiple_of(block * hid, 128), hid), :],
             preferred_element_type=f32,
         )
 
-    acc_ref[...] = down_block(0, me)
-    h_pass(0).wait_recv()
-    acc_ref[...] += down_block(chips, chip * CORES + 1 - core)
+    def block_step(part, step, multiply):
+        @pl.when(chip >= step)
+        def _():
+            t = chip - step
+            block_right(part, t).wait_recv()
+
+            @pl.when(chip < last)
+            def _():
+                block_right(part, t).start()
+
+            block_pass(part, t).start()
+            if multiply:
+                down_add(part, t * CORES + core)
+
+        @pl.when(chip + step <= last)
+        def _():
+            t = chip + step
+            block_left(part, t).wait_recv()
+
+            @pl.when(chip > 0)
+            def _():
+                block_left(part, t).start()
+
+            block_pass(part, t).start()
+            if multiply:
+                down_add(part, t * CORES + core)
+
+    up_load.wait()
+    up(0)
+    sum_step(0, 0)
+    up(1)
+    acc_ref[...] = jnp.zeros_like(acc_ref)
+    for step in range(1, last):
+        sum_step(0, step)
+    sum_end(0)
+    sum_step(1, 0)
+    for step in range(1, last):
+        block_step(0, step, False)
+        sum_step(1, step)
+    sum_end(1)
+    block_step(0, last, False)
+    load.wait()
+
+    @pl.loop(0, chips)
+    def _(t):
+        down_add(0, t * CORES + core)
+        block_pass(0, t).wait_recv()
+        down_add(0, t * CORES + 1 - core)
+
+    down_add(1, me)
 
     @pl.loop(1, chips)
     def _(step):
-        h_chip(step).wait_recv()
-        h_pass(step).start()
-        acc_ref[...] += down_block(step, behind(step) * CORES + core)
-        h_pass(step).wait_recv()
-        acc_ref[...] += down_block(chips + step, behind(step) * CORES + 1 - core)
+        block_step(1, step, True)
+
+    @pl.loop(0, chips)
+    def _(t):
+        block_pass(1, t).wait_recv()
+        down_add(1, t * CORES + 1 - core)
 
     back = {}
     for step in range(1, groups):
@@ -276,15 +436,28 @@
     for copies in (pair, far, spread, squares, back):
         for copy in copies.values():
             copy.wait_send()
-    h_pass(0).wait_send()
-    up_pair(0).wait_send()
-
-    @pl.loop(1, chips)
-    def _(step):
-        up_pair(step).wait_send()
-        up_chip(step).wait_send()
-        h_chip(step).wait_send()
-        h_pass(step).wait_send()
+    for part in range(2):
+
+        @pl.loop(0, chips)
+        def _(t):
+            up_pair(part, t).wait_send()
+            block_pass(part, t).wait_send()
+
+            @pl.when(t > chip)
+            def _():
+                sum_right(part, t).wait_send()
+
+            @pl.when(t < chip)
+            def _():
+                sum_left(part, t).wait_send()
+
+            @pl.when(jnp.logical_and(t <= chip, chip < last))
+            def _():
+                block_right(part, t).wait_send()
+
+            @pl.when(jnp.logical_and(t >= chip, chip > 0))
+            def _():
+                block_left(part, t).wait_send()
 
 
 def channel_mixer(partial_value, tokens, gain_share, w_up, w_down, chips, groups):
@@ -298,9 +471,10 @@
     return pl.pallas_call(
         functools.partial(mixer_kernel, chips, groups),
         out_shape=jax.ShapeDtypeStruct((rows, width), bf16),
-        in_specs=[spec] * 4 + [pl.BlockSpec(memory_space=pl.ANY)],
+        in_specs=[spec] * 3 + [pl.BlockSpec(memory_space=pl.ANY)] * 2,
         out_specs=spec,
         scratch_shapes=[
+            VMEM(w_up.shape, bf16),
             VMEM(w_down.shape, bf16),
             VMEM((chips, rows, width), bf16),
             VMEM((chips, rows, width), bf16),
@@ -310,19 +484,22 @@
             VMEM((ranks, 8, rows), f32),
             VMEM((chips, all_rows, hid), bf16),
             VMEM((chips, all_rows, hid), bf16),
+            VMEM((chips, all_rows, hid), f32),
             VMEM((chips, all_rows, hid), bf16),
             VMEM((chips, all_rows, hid), bf16),
-            VMEM((all_rows, hid), f32),
+            VMEM((chips, all_rows, hid), bf16),
+            VMEM((all_rows // 2, hid), f32),
             VMEM((ranks, all_rows, hid), bf16),
             VMEM((all_rows, width), f32),
             VMEM((groups, rows, width), bf16),
             VMEM((groups, rows, width), bf16),
             dma,
+            dma,
         ]
         + [dma((chips,))] * 4
         + [dma((groups,))] * 2
         + [dma((ranks,))] * 2
-        + [dma((chips,))] * 8
+        + [dma((2 * chips,))] * 12
         + [dma((groups,))] * 2,
         compiler_params=pltpu.CompilerParams(
             collective_id=1, has_side_effects=True, vmem_limit_bytes=48 * 1024 * 1024
@@ -465,23 +642,15 @@
     rows = tokens.shape[0]
     width_share = tokens.shape[1]
     head_count = w_query.shape[1] // HEAD_DIM
-    full_rows = gather_tp(tokens, chips)
-    full_f = full_rows.astype(jnp.float32)
-    normed = (
-        full_f * lax.rsqrt(jnp.mean(full_f * full_f, axis=-1, keepdims=True) + EPS) * mix_gain
-    ).astype(jnp.bfloat16)
-    proj = jnp.stack(
-        [
-            jnp.dot(normed, w, preferred_element_type=jnp.float32)
-            for w in (w_query, w_key, w_value, w_gate)
-        ]
-    ).reshape(4, rows * head_count, HEAD_DIM)
+    proj, rate_rows = project(
+        tokens, mix_gain[None, :], w_decay, w_beta, (w_query, w_key, w_value, w_gate), chips
+    )
+    proj = proj.reshape(rows, 4, head_count, HEAD_DIM).transpose(1, 0, 2, 3)
+    proj = proj.reshape(4, rows * head_count, HEAD_DIM)
     head_start = lax.axis_index("tp") * head_count
-    decay_cols = lax.dynamic_slice_in_dim(w_decay, head_start, head_count, 1)
-    beta_cols = lax.dynamic_slice_in_dim(w_beta, head_start, head_count, 1)
-    pre_decay = jnp.dot(normed, decay_cols, preferred_element_type=jnp.float32)
-    decay = jnp.exp(-decay_rate * jax.nn.softplus(pre_decay + decay_bias))
-    strength = jax.nn.sigmoid(jnp.dot(normed, beta_cols, preferred_element_type=jnp.float32))
+    rate_rows = lax.dynamic_slice_in_dim(rate_rows, head_start, head_count, 2)
+    decay = jnp.exp(-decay_rate * jax.nn.softplus(rate_rows[0] + decay_bias))
+    strength = jax.nn.sigmoid(rate_rows[1])
     rates = jnp.stack([decay, strength], axis=-1).reshape(rows * head_count, 2)
     new_state, head_out = update_state(proj, rates, out_gain[None, :], state)
     head_out = head_out.reshape(rows, head_count * HEAD_DIM)

time: 157 us -> 156 us (level)
  the two profiles are of different devices: /device:TPU:24 before, /device:TPU:0 now
where the time goes in v3:
time: 156 us; the launch traced here: 155 us
  Pallas kernels  129 us (83%)
  local copies, waits for them, and re-layouts  23.1 us (15%)
  other arithmetic  1.62 us (1%)
    pallas_call x1, Pallas kernels, channel_mixer(): pl.pallas_call(functools.partial(mixer_kernel, chips, groups), out_shape=...  103 us
    unnamed x29, local copies, waits for them, and re-layouts  18.6 us
    pallas_call x1, Pallas kernels, project(): pl.pallas_call(functools.partial(project_kernel, chips), out_shape=(jax.S...  15.7 us
    pallas_call x1, Pallas kernels, update_state(): pl.pallas_call(functools.partial(state_kernel, heads), grid=(rows // bloc...  10.8 us

profile of v3, /device:TPU:0, one launch (start us, length us, event | category | flops | bytes accessed | tf_op | source)
XLA Modules:
  0.0 155.4 jit_solution(860362378779312163)
XLA Ops:
  0.6 0.0 copy-start
  0.6 0.0 copy-start.11
  0.7 1.6 %copy.34.decay_ref = bf16[4096,32]{1,0:T(8,128)(2,1)S(1)} copy(bf16[4096,32]{0,1:T(8,128)(2,1)} %param.22) | data formatting | bytes 524288 | tf_op args[6]
  2.2 2.3 %copy.35.beta_ref = bf16[4096,32]{1,0:T(8,128)(2,1)} copy(bf16[4096,32]{0,1:T(8,128)(2,1)} %param.23) | data formatting | bytes 524288 | tf_op args[7]
  4.5 0.0 copy-done.11
  4.5 0.0 copy-start.3
  4.5 1.2 copy-done.3
  5.7 0.0 copy-start.4
  5.7 1.6 %copy-done.4 = bf16[4096,256]{1,0:T(8,128)(2,1)S(1)} copy-done((bf16[4096,256]{1,0:T(8,128)(2,1)S(1)}, bf16[4096,256]{1,0:T(8,128)(2,1)}, u32[]{:S(2)}) %copy-start.4) | copy-done | bytes 2097176
  7.3 0.0 copy-start.5
  7.3 1.6 %copy-done.5 = bf16[4096,256]{1,0:T(8,128)(2,1)S(1)} copy-done((bf16[4096,256]{1,0:T(8,128)(2,1)S(1)}, bf16[4096,256]{1,0:T(8,128)(2,1)}, u32[]{:S(2)}) %copy-start.5) | copy-done | bytes 2097176
  8.9 0.0 copy-start.6
  8.9 1.6 %copy-done.6 = bf16[4096,256]{1,0:T(8,128)(2,1)S(1)} copy-done((bf16[4096,256]{1,0:T(8,128)(2,1)S(1)}, bf16[4096,256]{1,0:T(8,128)(2,1)}, u32[]{:S(2)}) %copy-start.6) | copy-done | bytes 2097176
  10.5 0.0 copy-start.7
  10.5 1.6 %copy-done.7 = bf16[4096,256]{1,0:T(8,128)(2,1)S(1)} copy-done((bf16[4096,256]{1,0:T(8,128)(2,1)S(1)}, bf16[4096,256]{1,0:T(8,128)(2,1)}, u32[]{:S(2)}) %copy-start.7) | copy-done | bytes 2097176
  12.1 0.0 copy-start.8
  12.1 0.9 copy-done.8
  13.0 15.7 %project.1 = (f32[96,1024]{1,0:T(8,128)S(1)}, f32[2,96,32]{2,1,0:T(8,128)S(1)}) custom-call(bf16[96,512]{1,0:T(8,128)(2,1)S(1)} %copy-done.8, f32[1,4096]{1,0:T(1,128)S(1)} %bitcast.14, bf16[4096,32]{1,0:T(8,128)(2,1)S(1)} %copy.34.decay_ref, bf16[4096,32]{1,0:T(8,128)(2,1)S(1)} %copy-done.3, bf16[4096,256]{1,0:T(8,128)(2,1)S(1)} %copy-done.4, ...), custom_call_target="tpu_custom_call" | custom-call | tf_op jit(solution)/shard_map/project/pallas_call | solution.py:131
  28.7 0.0 copy-start.10
  28.7 0.6 copy-done.10
  29.3 0.0 copy-start.12
  29.3 0.9 constant_dynamic-slice_fusion
  30.3 0.1 squeeze.4
  30.4 0.7 neg.27
  31.0 0.1 mul.25
  31.1 0.7 add.49
  31.8 0.1 add.50
  32.0 0.1 div.15
  32.1 0.1 copy.40.rates_ref
  32.2 1.0 copy.36
  33.2 1.4 copy.37
  34.6 0.0 copy-done.12
  34.6 0.0 copy-start.1
  34.6 2.8 %copy-done.1 = f32[96,4,4096]{2,1,0:T(4,128)S(1)} copy-done((f32[96,4,4096]{2,1,0:T(4,128)S(1)}, f32[96,4,4096]{2,1,0:T(4,128)}, u32[]{:S(2)}) %copy-start.1) | copy-done | bytes 6291480
  37.4 10.8 %update_state.1 = (f32[96,4,4096]{2,1,0:T(4,128)}, bf16[384,64]{1,0:T(8,128)(2,1)S(1)}) custom-call(f32[4,384,64]{2,1,0:T(8,128)S(1)} %bitcast.13, f32[384,2]{1,0:T(8,128)S(1)} %copy.40.rates_ref, f32[1,64]{1,0:T(1,128)S(1)} %bitcast.16, f32[96,4,4096]{2,1,0:T(4,128)S(1)} %copy-done.1), custom_call_target="tpu_custom_call" | custom-call | tf_op jit(solution)/shard_map/update_state/pallas_call | solution.py:593
  48.2 0.0 copy-start.9
  48.2 0.1 reshape.113
  48.3 0.0 copy-done
  48.3 0.5 convolution_convert_fusion.part_ref
  48.8 0.8 dynamic_slice.7
  49.6 0.0 copy-done.9
  49.6 0.0 copy-start.2
  49.6 2.2 %copy-done.2 = bf16[512,4096]{1,0:T(8,128)(2,1)S(1)} copy-done((bf16[512,4096]{1,0:T(8,128)(2,1)S(1)}, bf16[512,4096]{1,0:T(8,128)(2,1)}, u32[]{:S(2)}) %copy-start.2) | copy-done | bytes 4194328
  51.7 103.0 %channel_mixer.1 = bf16[96,512]{1,0:T(8,128)(2,1)S(1)} custom-call(bf16[96,4096]{1,0:T(8,128)(2,1)S(1)} %convolution_convert_fusion.part_ref, bf16[96,512]{1,0:T(8,128)(2,1)S(1)} %copy-done.9, f32[1,512]{1,0:T(1,128)S(1)} %bitcast.15, bf16[512,4096]{1,0:T(8,128)(2,1)S(1)} %copy-done.2, bf16[4096,512]{1,0:T(8,128)(2,1)} %down_hbm.1), custom_call_target="tpu_custom_call" | custom-call | tf_op jit(solution)/shard_map/channel_mixer/pallas_call | solution.py:471
  154.8 0.6 copy.42
  (3 shorter events, 0.0 us)
Async XLA Ops:
  0.6 47.7 %copy-start = (bf16[256,4096]{1,0:T(8,128)(2,1)S(1)}, bf16[256,4096]{1,0:T(8,128)(2,1)}, u32[]{:S(2)}) copy-start(bf16[256,4096]{1,0:T(8,128)(2,1)} %param.28) | copy-start | bytes 6291460
  0.6 3.9 %copy-start.11 = (f32[4096]{0:T(1024)S(1)}, f32[4096]{0:T(1024)}, u32[]{:S(2)}) copy-start(f32[4096]{0:T(1024)} %param.26) | copy-start | bytes 49156
  4.5 1.2 copy-start.3
  5.7 1.6 %copy-start.4 = (bf16[4096,256]{1,0:T(8,128)(2,1)S(1)}, bf16[4096,256]{1,0:T(8,128)(2,1)}, u32[]{:S(2)}) copy-start(bf16[4096,256]{1,0:T(8,128)(2,1)} %wq_hbm.1) | copy-start | bytes 6291460
  7.3 1.6 %copy-start.5 = (bf16[4096,256]{1,0:T(8,128)(2,1)S(1)}, bf16[4096,256]{1,0:T(8,128)(2,1)}, u32[]{:S(2)}) copy-start(bf16[4096,256]{1,0:T(8,128)(2,1)} %wk_hbm.1) | copy-start | bytes 6291460
  8.9 1.6 %copy-start.6 = (bf16[4096,256]{1,0:T(8,128)(2,1)S(1)}, bf16[4096,256]{1,0:T(8,128)(2,1)}, u32[]{:S(2)}) copy-start(bf16[4096,256]{1,0:T(8,128)(2,1)} %wv_hbm.1) | copy-start | bytes 6291460
  10.5 1.6 %copy-start.7 = (bf16[4096,256]{1,0:T(8,128)(2,1)S(1)}, bf16[4096,256]{1,0:T(8,128)(2,1)}, u32[]{:S(2)}) copy-start(bf16[4096,256]{1,0:T(8,128)(2,1)} %wg_hbm.1) | copy-start | bytes 6291460
  12.1 0.9 copy-start.8
  28.7 0.6 copy-start.10
  29.3 5.3 %copy-start.12 = (f32[64]{0:T(128)S(1)}, f32[64]{0:T(128)}, u32[]{:S(2)}) copy-start(f32[64]{0:T(128)} %param.27) | copy-start | bytes 772
  34.6 2.8 %copy-start.1 = (f32[96,4,4096]{2,1,0:T(4,128)S(1)}, f32[96,4,4096]{2,1,0:T(4,128)}, u32[]{:S(2)}) copy-start(f32[96,4,4096]{2,1,0:T(4,128)} %state_ref.1) | copy-start | bytes 18874372
  48.2 1.4 copy-start.9
  49.6 2.2 %copy-start.2 = (bf16[512,4096]{1,0:T(8,128)(2,1)S(1)}, bf16[512,4096]{1,0:T(8,128)(2,1)}, u32[]{:S(2)}) copy-start(bf16[512,4096]{1,0:T(8,128)(2,1)} %up_hbm.1) | copy-start | bytes 12582916
